TPU v7x, 32 devices: a whole 2x2x4 slice. The times are simulated.
32 devices in a mesh: sp: 8 (over z, core), tp: 4 (over y, x).
Axes of the slice: x: 2, y: 2, z: 4, core: 2. Of those that a mesh axis runs over, the one named last changes fastest.
Arguments:
- tokens: bfloat16 [2048, 1024], P('sp', 'tp'), may hold values from -6 to 6
- norm_gain: bfloat16 [2, 1024], P(None, 'tp'), may hold values from 0.099609375 to 1.8984375
- query_weight: bfloat16 [2, 1024, 1024], P(None, 'sp', 'tp'), may hold values from -0.1875 to 0.1875
- key_weight: bfloat16 [2, 1024, 1024], P(None, 'sp', 'tp'), may hold values from -0.1875 to 0.1875
- value_weight: bfloat16 [2, 1024, 1024], P(None, 'sp', 'tp'), may hold values from -0.1875 to 0.1875
- output_weight: bfloat16 [2, 1024, 1024], P(None, 'tp', 'sp'), may hold values from -0.5 to 0.5
- offset_bias: float32 [2, 16, 15, 31], P(None, 'tp'), may hold values from -4 to 4
Outputs:
- mixed: bfloat16 [2048, 1024], P('sp', 'tp')
All inputs are finite; a program needn't handle non-finite values.
Results may differ from a plain program's by a relative error of at most 0.03.
Values may be sent and summed in bfloat16 or wider, within the bound.
A program may use at most 64 MiB of HBM per device.

v0:
```python
import jax
import jax.numpy as jnp
from jax import lax
from jax.sharding import PartitionSpec as P

HEAD_DIM = 64
WIN_H = 8
WIN_W = 16
ROWS_DEV = 4
COLS = 64
D = 1024
norm_eps = 1e-06


def folded(value, axis, dim, update, carry):
    whole = jax.tree.map(lambda part: lax.all_gather(part, axis, axis=dim, tiled=True), value)
    return update(carry, whole, jnp.int32(0))


def extended(block, sides, width, periodic):
    for axis, dim in sides:
        count = lax.axis_size(axis)
        forward = [(i, i + 1) for i in range(count - 1)]
        if periodic:
            forward.append((count - 1, 0))
        backward = [(target, source) for source, target in forward]
        low = lax.ppermute(
            lax.slice_in_dim(block, block.shape[dim] - width, None, axis=dim), axis, forward
        )
        high = lax.ppermute(lax.slice_in_dim(block, 0, width, axis=dim), axis, backward)
        block = jnp.concatenate([low, block, high], axis=dim)
    return block


def own_rows(portion, rows, axis):
    count = rows * lax.axis_size(axis)
    sent = portion(jnp.int32(0), count).astype(jnp.bfloat16)
    return lax.psum_scatter(sent, axis, scatter_dimension=0, tiled=True).astype(jnp.float32)


def attend(query, padded, table, base, total_rows):
    heads = table.shape[0]
    local_width = heads * HEAD_DIM
    half = WIN_H // 2
    span_rows = ROWS_DEV + WIN_H
    glob = base + jnp.arange(ROWS_DEV, dtype=jnp.int32)
    first = jnp.clip(glob - half, 0, total_rows - WIN_H).astype(jnp.int32)
    local_first = first - base + half
    padded_row = jnp.arange(span_rows, dtype=jnp.int32)
    row_inside = (padded_row[None, :] >= local_first[:, None]) & (
        padded_row[None, :] < local_first[:, None] + WIN_H
    )
    row_offset = padded_row[None, :] + base - half - glob[:, None] + (WIN_H - 1)
    row_codes = jnp.arange(2 * WIN_H - 1, dtype=jnp.int32)
    row_onehot = (row_offset[:, :, None] == row_codes[None, None, :]).astype(jnp.float32)
    column = jnp.arange(COLS, dtype=jnp.int32)
    col_start = jnp.clip(column - WIN_W // 2, 0, COLS - WIN_W).astype(jnp.int32)
    col_inside = (column[None, :] >= col_start[:, None]) & (
        column[None, :] < col_start[:, None] + WIN_W
    )
    col_offset = column[None, :] - column[:, None] + (WIN_W - 1)
    col_codes = jnp.arange(2 * WIN_W - 1, dtype=jnp.int32)
    col_onehot = (col_offset[:, :, None] == col_codes[None, None, :]).astype(jnp.float32)
    bias = jnp.einsum(
        "hab,ria,qkb->rhqik", table, row_onehot, col_onehot, precision=lax.Precision.HIGHEST
    )
    inside = row_inside[:, None, None, :, None] & col_inside[None, None, :, None, :]
    keys = padded[:, :, :local_width].reshape(span_rows, COLS, heads, HEAD_DIM)
    values = padded[:, :, local_width:].reshape(span_rows, COLS, heads, HEAD_DIM)
    grid_query = query.reshape(ROWS_DEV, COLS, heads, HEAD_DIM)
    score = jnp.einsum(
        "rqhd,ikhd->rhqik", grid_query, keys, preferred_element_type=jnp.float32
    ) * HEAD_DIM ** (-0.5)
    score = jnp.where(inside, score + bias, -1e30)
    flat = score.reshape(ROWS_DEV, heads, COLS, span_rows * COLS)
    weights = jax.nn.softmax(flat, axis=-1).reshape(score.shape).astype(jnp.bfloat16)
    out = jnp.einsum(
        "rhqik,ikhd->rqhd", weights, values, preferred_element_type=jnp.float32
    ).astype(jnp.bfloat16)
    return out.reshape(ROWS_DEV * COLS, local_width)


def body(tokens, norm_gain, query_weight, key_weight, value_weight, output_weight, offset_bias):
    layers = query_weight.shape[0]
    local_width = query_weight.shape[2]
    feature_rows = tokens.shape[1]
    token_count = tokens.shape[0]
    half = WIN_H // 2
    base = lax.axis_index("sp") * ROWS_DEV
    total_rows = ROWS_DEV * lax.axis_size("sp")
    every = (
        lax.all_gather(query_weight, "sp", axis=1, tiled=True),
        lax.all_gather(key_weight, "sp", axis=1, tiled=True),
        lax.all_gather(value_weight, "sp", axis=1, tiled=True),
        lax.all_gather(output_weight, "sp", axis=2, tiled=True),
    )
    current = tokens
    for layer in range(layers):
        query_full = every[0][layer]
        key_full = every[1][layer]
        value_full = every[2][layer]
        output_full = every[3][layer]
        stacked = jnp.concatenate([query_full, key_full, value_full], axis=1)
        floats = current.astype(jnp.float32)
        squares = lax.psum(jnp.sum(floats * floats, axis=1), "tp")
        factor = lax.rsqrt(squares / D + norm_eps)
        normed = (floats * factor[:, None] * norm_gain[layer].astype(jnp.float32)).astype(
            jnp.bfloat16
        )
        table = offset_bias[layer].astype(jnp.float32)

        def project(carry, piece, start):
            weight_rows = lax.dynamic_slice_in_dim(stacked, start, piece.shape[1], 0)
            return carry + jnp.dot(piece, weight_rows, preferred_element_type=jnp.float32)

        projected = folded(
            normed, "tp", 1, project, jnp.zeros((token_count, 3 * local_width), jnp.float32)
        ).astype(jnp.bfloat16)
        query = projected[:, :local_width]
        pair = projected[:, local_width:].reshape(ROWS_DEV, COLS, 2 * local_width)
        padded = extended(pair, (("sp", 0),), half, False)
        attended = attend(query, padded, table, base, total_rows)

        def project_out(start, count):
            weight_cols = lax.dynamic_slice_in_dim(output_full, start, count, 1)
            return lax.dot_general(
                weight_cols, attended, (((0,), (1,)), ((), ())), preferred_element_type=jnp.float32
            )

        summed = own_rows(project_out, feature_rows, "tp")
        current = summed.T.astype(jnp.bfloat16)
    return current


def solution(mesh):
    in_specs = (
        P("sp", "tp"),
        P(None, "tp"),
        P(None, "sp", "tp"),
        P(None, "sp", "tp"),
        P(None, "sp", "tp"),
        P(None, "tp", "sp"),
        P(None, "tp", None, None),
    )
    out_specs = P("sp", "tp")
    return jax.shard_map(body, mesh=mesh, in_specs=in_specs, out_specs=out_specs, check_vma=False)
```

profile of v0, /device:TPU:0, one launch (start us, length us, event | category | flops | bytes accessed | tf_op | source)
XLA Modules:
  0.0 223.2 jit_solution(17769417152890954253)
XLA Ops:
  6.5 0.7 all-gather.9.cloned.1.call-update
  7.3 0.7 all-gather.5.cloned.1.call-update
  8.1 0.7 all-gather.7.cloned.1.call-update
  8.8 0.5 all-gather.11.cloned.1.call-update
  9.4 0.8 slice_convert_fusion
  10.2 1.0 fusion.59
  11.2 11.4 %psum.14 = f32[256]{0:T(256)S(1)} all-reduce(f32[256]{0:T(256)S(1)} %fusion.59), channel_id=1, replica_groups=mesh['sp'=8,'tp'=4] {'tp'}, use_global_device_ids=true, to_apply=%region_1.0 | all-reduce | flops 256 | bytes 2048 | tf_op jit(solution)/shard_map/psum | solution.py:105
  22.6 1.0 fusion.61
  23.6 11.2 %all_gather.18 = bf16[256,1024]{1,0:T(8,128)(2,1)S(1)} all-gather(bf16[256,256]{1,0:T(8,128)(2,1)S(1)} %fusion.61), channel_id=1, replica_groups=mesh['sp'=8,'tp'=4] {'tp'}, dimensions={1}, use_global_device_ids=true | all-gather | bytes 655360 | tf_op jit(solution)/shard_map/all_gather | solution.py:16
  35.0 1.4 fusion.79
  36.4 1.0 fusion.53
  37.5 5.7 %fusion.10 = f32[64,64,4,4,12]{1,4,3,2,0:T(8,128)} fusion(f32[64,64,4,15]{1,3,2,0:T(8,128)S(1)} %fusion.53, s32[4,12]{1,0:T(4,128)S(1)} %subtract_add_fusion.1), kind=kOutput, calls=%fused_computation.16 | convolution fusion | flops 141558480 | bytes 4128960 | tf_op jit(solution)/shard_map/hab,ria,qkb->rhqik/dot_general | solution.py:64
  43.2 2.1 slice_bitcast_fusion.2
  45.2 12.2 %all-gather.5.cloned.1.call-done = bf16[2,1024,256]{2,1,0:T(8,128)(2,1)} async-done(((bf16[2,128,256]{2,1,0:T(8,128)(2,1)}), bf16[2,1024,256]{2,1,0:T(8,128)(2,1)}) %all-gather.5.cloned.1.call-update) | async-done | bytes 1048592 | tf_op jit(solution)/shard_map/all_gather | solution.py:92
  57.4 2.1 slice_bitcast_fusion.4
  59.5 21.4 %all-gather.7.cloned.1.call-done = bf16[2,1024,256]{2,1,0:T(8,128)(2,1)} async-done(((bf16[2,128,256]{2,1,0:T(8,128)(2,1)}), bf16[2,1024,256]{2,1,0:T(8,128)(2,1)}) %all-gather.7.cloned.1.call-update) | async-done | bytes 1048592 | tf_op jit(solution)/shard_map/all_gather | solution.py:93
  80.9 2.1 slice_bitcast_fusion.3
  83.0 0.6 fusion.27
  83.6 2.1 collective-permute-start
  85.7 1.3 collective-permute-start.1
  87.0 9.8 %copy.30 = f32[64,64,4,4,12]{0,1,3,4,2:T(8,128)} copy(f32[64,64,4,4,12]{1,4,3,2,0:T(8,128)} %fusion.10) | data formatting | bytes 6291456 | tf_op jit(solution)/shard_map/hab,ria,qkb->rhqik/dot_general | solution.py:64
  96.8 0.2 broadcast_and_fusion
  97.5 0.3 reshape.197
  97.8 0.3 reshape.196
  98.1 4.5 %fusion.80 = (f32[4,4,64]{2,0,1:T(4,128)S(1)}, f32[4,4,64,12,64]{2,4,0,3,1:T(8,128)S(1)}) fusion(f32[64,64,4,4,12]{0,1,3,4,2:T(8,128)} %copy.30, bf16[4,64,4,64,1]{3,2,1,0,4:T(4,128)(2,1)S(1)} %bitcast.99, bf16[12,64,4,64,1]{3,2,1,0,4:T(4,128)(2,1)S(1)} %bitcast.97, pred[4,64,12,64]{1,3,0,2:T(8,128)(4,1)S(1)} %broadcast_and_fusion), kind=kOutput, calls=%fused_computation.106 | convolution fusion | flops 103808000 | bytes 7016448 | tf_op jit(solution)/shard_map/rqhd,ikhd->rhqik/dot_general | solution.py:71
  102.7 1.0 fusion.2
  103.7 1.2 fusion.44
  105.3 1.3 all-gather.11.cloned.1.call-done
  106.6 2.1 fusion.36
  108.8 1.8 fusion.51
  110.6 23.9 %reduce-scatter.3.cloned.1.call-done = bf16[256,256]{0,1:T(8,128)(2,1)} async-done(((bf16[1024,256]{0,1:T(8,128)(2,1)}), bf16[256,256]{0,1:T(8,128)(2,1)}) %reduce-scatter.3.cloned.1.call-update) | async-done | bytes 131088 | tf_op jit(solution)/shard_map/reduce_scatter | solution.py:38
  134.6 1.0 fusion.62
  135.6 9.1 %psum.15 = f32[256]{0:T(256)S(1)} all-reduce(f32[256]{0:T(256)S(1)} %fusion.62), channel_id=1, replica_groups=mesh['sp'=8,'tp'=4] {'tp'}, use_global_device_ids=true, to_apply=%region_6.7 | all-reduce | flops 256 | bytes 2048 | tf_op jit(solution)/shard_map/psum | solution.py:105
  144.7 1.0 fusion.67
  145.7 12.1 %all_gather.23 = bf16[256,1024]{1,0:T(8,128)(2,1)S(1)} all-gather(bf16[256,256]{1,0:T(8,128)(2,1)S(1)} %fusion.67), channel_id=1, replica_groups=mesh['sp'=8,'tp'=4] {'tp'}, dimensions={1}, use_global_device_ids=true | all-gather | bytes 655360 | tf_op jit(solution)/shard_map/all_gather | solution.py:16
  157.8 2.0 fusion.24
  159.8 1.3 collective-permute-start.2
  161.1 1.3 collective-permute-start.3
  162.4 5.7 %fusion.8 = f32[64,64,4,4,12]{1,4,3,2,0:T(8,128)} fusion(f32[64,64,4,15]{1,3,2,0:T(8,128)S(1)} %fusion.51, s32[4,12]{1,0:T(4,128)S(1)} %subtract_add_fusion.1), kind=kOutput, calls=%fused_computation.14 | convolution fusion | flops 141558480 | bytes 4128960 | tf_op jit(solution)/shard_map/hab,ria,qkb->rhqik/dot_general | solution.py:64
  168.1 9.8 %copy.38 = f32[64,64,4,4,12]{0,1,3,4,2:T(8,128)} copy(f32[64,64,4,4,12]{1,4,3,2,0:T(8,128)} %fusion.8) | data formatting | bytes 6291456 | tf_op jit(solution)/shard_map/hab,ria,qkb->rhqik/dot_general | solution.py:64
  178.0 1.0 pad_maximum_fusion.1
  179.2 0.3 reshape.202
  179.5 0.3 reshape.201
  179.8 4.5 %fusion.81 = (f32[4,4,64]{2,0,1:T(4,128)S(1)}, f32[4,4,64,12,64]{2,4,0,3,1:T(8,128)S(1)}) fusion(f32[64,64,4,4,12]{0,1,3,4,2:T(8,128)} %copy.38, bf16[4,64,4,64,1]{3,2,1,0,4:T(4,128)(2,1)S(1)} %bitcast.98, bf16[12,64,4,64,1]{3,2,1,0,4:T(4,128)(2,1)S(1)} %bitcast.96, pred[4,64,12,64]{1,3,0,2:T(8,128)(4,1)S(1)} %broadcast_and_fusion), kind=kOutput, calls=%fused_computation.107 | convolution fusion | flops 103808000 | bytes 7016448 | tf_op jit(solution)/shard_map/rqhd,ikhd->rhqik/dot_general | solution.py:71
  184.3 1.0 fusion.3
  185.4 1.2 fusion.47
  187.0 1.1 fusion.37
  188.1 28.2 %reduce-scatter.5.cloned.1.call-done = bf16[256,256]{0,1:T(8,128)(2,1)} async-done(((bf16[1024,256]{0,1:T(8,128)(2,1)}), bf16[256,256]{0,1:T(8,128)(2,1)}) %reduce-scatter.5.cloned.1.call-update) | async-done | bytes 131088 | tf_op jit(solution)/shard_map/reduce_scatter | solution.py:38
  (39 shorter events, 2.0 us)
Async XLA Ops:
  6.5 36.6 %all-gather.9.cloned.1.call-start = ((), (), s32[]{:S(2)}) async-start(), calls=%async_computation.4 | async-start | bytes 1179648 | tf_op jit(solution)/shard_map/all_gather | solution.py:94
  7.3 50.2 %all-gather.5.cloned.1.call-start = ((), (), s32[]{:S(2)}) async-start(), calls=%async_computation.2 | async-start | bytes 1179648 | tf_op jit(solution)/shard_map/all_gather | solution.py:92
  8.0 72.9 %all-gather.7.cloned.1.call-start = ((), (), s32[]{:S(2)}) async-start(), calls=%async_computation.3 | async-start | bytes 1179648 | tf_op jit(solution)/shard_map/all_gather | solution.py:93
  8.7 97.9 %all-gather.11.cloned.1.call-start = ((), (), s32[]{:S(2)}) async-start(), calls=%async_computation.5 | async-start | bytes 1179648 | tf_op jit(solution)/shard_map/all_gather | solution.py:95
  9.3 125.2 %reduce-scatter.3.cloned.1.call-start = ((), (), s32[]{:S(2)}) async-start(), calls=%async_computation.6 | async-start | bytes 655360 | tf_op jit(solution)/shard_map/reduce_scatter | solution.py:38
  83.6 13.7 %collective-permute-start = (bf16[4,64,512]{2,1,0:T(8,128)(2,1)S(1)}, bf16[4,64,512]{2,1,0:T(8,128)(2,1)S(1)}, u32[]{:S(2)}, u32[]{:S(2)}) collective-permute-start(bf16[4,64,512]{2,1,0:T(8,128)(2,1)S(1)} %bitcast.100), channel_id=1, source_target_pairs={{0,4},{4,8},{8,12},{12,16},{16,20},{20,24},{24,28},{1,5},{5,9},{9,... | collective-permute-start | bytes 786440 | tf_op jit(solution)/shard_map/ppermute | solution.py:27
  85.7 11.6 %collective-permute-start.1 = (bf16[4,64,512]{2,1,0:T(8,128)(2,1)S(1)}, bf16[4,64,512]{2,1,0:T(8,128)(2,1)S(1)}, u32[]{:S(2)}, u32[]{:S(2)}) collective-permute-start(bf16[4,64,512]{2,1,0:T(8,128)(2,1)S(1)} %bitcast.101), channel_id=1, source_target_pairs={{4,0},{8,4},{12,8},{16,12},{20,16},{24,20},{28,24},{5,1},{9,5},{13... | collective-permute-start | bytes 786440 | tf_op jit(solution)/shard_map/ppermute | solution.py:30
  108.8 107.6 %reduce-scatter.5.cloned.1.call-start = ((), (), s32[]{:S(2)}) async-start(), calls=%async_computation.7 | async-start | bytes 655360 | tf_op jit(solution)/shard_map/reduce_scatter | solution.py:38
  159.8 18.2 %collective-permute-start.2 = (bf16[4,64,512]{2,1,0:T(8,128)(2,1)S(1)}, bf16[4,64,512]{2,1,0:T(8,128)(2,1)S(1)}, u32[]{:S(2)}, u32[]{:S(2)}) collective-permute-start(bf16[4,64,512]{2,1,0:T(8,128)(2,1)S(1)} %bitcast.103), channel_id=1, source_target_pairs={{0,4},{4,8},{8,12},{12,16},{16,20},{20,24},{24,28},{1,5},{5,9},{9,... | collective-permute-start | bytes 786440 | tf_op jit(solution)/shard_map/ppermute | solution.py:27
  161.1 16.9 %collective-permute-start.3 = (bf16[4,64,512]{2,1,0:T(8,128)(2,1)S(1)}, bf16[4,64,512]{2,1,0:T(8,128)(2,1)}, u32[]{:S(2)}, u32[]{:S(2)}) collective-permute-start(bf16[4,64,512]{2,1,0:T(8,128)(2,1)S(1)} %bitcast.104), channel_id=1, source_target_pairs={{4,0},{8,4},{12,8},{16,12},{20,16},{24,20},{28,24},{5,1},{9,5},{13... | collective-permute-start | bytes 786440 | tf_op jit(solution)/shard_map/ppermute | solution.py:30
  185.4 1.6 copy-start
Sparse Core Ops, SparseCore 0:
  8.9 24.9 all-gather.8
  35.5 21.8 all-gather.4
  59.0 21.8 all-gather.6
  82.3 24.2 all-gather.10
  109.3 25.2 reduce-scatter.2
  188.2 28.0 reduce-scatter.4
where the time goes:
time: 224 us; the launch traced here: 223 us
  waiting for transfers between devices  89.7 us (40%)
  blocking collectives  43.8 us (20%)
  matrix products  31.3 us (14%)
  local copies, waits for them, and re-layouts  29.8 us (13%)
  between operations  13.8 us (6%)
  other arithmetic  8.54 us (4%)
  starting transfers between devices  6.23 us (3%)
    reduce_scatter x2, waiting for transfers between devices, own_rows(): lax.psum_scatter(sent, axis, scatter_dimension=0, tiled=True)  52.2 us
    all_gather x2, blocking collectives, folded(): lax.all_gather(part, axis, axis=dim, tiled=True)  23.3 us
    all_gather x1, waiting for transfers between devices, body(): lax.all_gather(key_weight, 'sp', axis=1, tiled=True)  21.4 us
    psum x2, blocking collectives, body(): squares = lax.psum(jnp.sum(floats * floats, axis=1), 'tp')  20.5 us
    dot_general x2, local copies, waits for them, and re-layouts, attend(): jnp.einsum('hab,ria,qkb->rhqik', table, row_onehot, col_onehot, precision...  19.6 us
    dot_general x4, matrix products, attend(): jnp.einsum('hab,ria,qkb->rhqik', table, row_onehot, col_onehot, precision...  14.1 us
    all_gather x1, waiting for transfers between devices, body(): lax.all_gather(query_weight, 'sp', axis=1, tiled=True)  12.2 us
    dot_general x2, matrix products, attend(): jnp.einsum('rqhd,ikhd->rhqik', grid_query, keys, preferred_element_type=j...  9.06 us
  transfers between devices with their start and end apart: 10, of which 5 were waited for; matrix products, arithmetic and copies ran while one was open for 24% of the time, Pallas kernels for 0%

commit v1 on v0

--- a/solution.py
+++ b/solution.py
@@ -102,7 +102,7 @@
         output_full = every[3][layer]
         stacked = jnp.concatenate([query_full, key_full, value_full], axis=1)
         floats = current.astype(jnp.float32)
-        squares = lax.psum(jnp.sum(floats * floats, axis=1), "tp")
+        squares = jnp.sum(lax.all_gather(jnp.sum(floats * floats, axis=1), "tp"), axis=0)
         factor = lax.rsqrt(squares / D + norm_eps)
         normed = (floats * factor[:, None] * norm_gain[layer].astype(jnp.float32)).astype(
             jnp.bfloat16

time: 224 us -> 222 us (level)
  blocking collectives: 43.8 us -> 41.1 us
  waiting for transfers between devices: 89.7 us -> 92.1 us
    psum x2 -> x0, blocking collectives: 20.5 us -> none  [body(): squares = lax.psum(jnp.sum(floats * floats, axis=1), 'tp')]
    all_gather x0 -> x2, blocking collectives: none -> 17.6 us  [body(): lax.all_gather(jnp.sum(floats * floats, axis=1), 'tp')]
  transfers between devices with their start and end apart: 10 -> 10, of which waited for: 5 -> 5; matrix products, arithmetic and copies ran while one was open for 24% -> 23% of each run, Pallas kernels for 0% -> 0%
where the time goes in v1:
time: 222 us; the launch traced here: 221 us
  waiting for transfers between devices  92.1 us (41%)
  blocking collectives  41.1 us (19%)
  matrix products  30.4 us (14%)
  local copies, waits for them, and re-layouts  29.2 us (13%)
  between operations  13.8 us (6%)
  other arithmetic  8.45 us (4%)
  starting transfers between devices  6.23 us (3%)
    reduce_scatter x2, waiting for transfers between devices, own_rows(): lax.psum_scatter(sent, axis, scatter_dimension=0, tiled=True)  52.9 us
    all_gather x2, blocking collectives, folded(): lax.all_gather(part, axis, axis=dim, tiled=True)  23.5 us
    all_gather x1, waiting for transfers between devices, body(): lax.all_gather(key_weight, 'sp', axis=1, tiled=True)  21.4 us
    dot_general x2, local copies, waits for them, and re-layouts, attend(): jnp.einsum('hab,ria,qkb->rhqik', table, row_onehot, col_onehot, precision...  19.6 us
    all_gather x2, blocking collectives, body(): lax.all_gather(jnp.sum(floats * floats, axis=1), 'tp')  17.6 us
    all_gather x1, waiting for transfers between devices, body(): lax.all_gather(query_weight, 'sp', axis=1, tiled=True)  13.8 us
    dot_general x4, matrix products, attend(): jnp.einsum('hab,ria,qkb->rhqik', table, row_onehot, col_onehot, precision...  13.3 us
    dot_general x2, matrix products, attend(): jnp.einsum('rqhd,ikhd->rhqik', grid_query, keys, preferred_element_type=j...  9.06 us
  transfers between devices with their start and end apart: 10, of which 5 were waited for; matrix products, arithmetic and copies ran while one was open for 23% of the time, Pallas kernels for 0%

profile of v1, /device:TPU:0, one launch (start us, length us, event | category | flops | bytes accessed | tf_op | source)
XLA Modules:
  0.0 221.4 jit_solution(12100841044575629911)
XLA Ops:
  6.5 0.7 all-gather.13.cloned.1.call-update
  7.3 0.7 all-gather.9.cloned.1.call-update
  8.1 0.7 all-gather.11.cloned.1.call-update
  8.8 0.5 all-gather.15.cloned.1.call-update
  9.4 0.8 slice_convert_fusion
  10.2 1.0 fusion.61
  11.2 9.6 %all-gather.2 = f32[4,1,256]{2,1,0:T(1,128)S(1)} all-gather(f32[1,1,256]{2,1,0:T(1,128)S(1)} %bitcast.113), channel_id=2, replica_groups=mesh['sp'=8,'tp'=4] {'tp'}, dimensions={0}, use_global_device_ids=true | all-gather | bytes 5120 | tf_op jit(solution)/shard_map/all_gather | solution.py:105
  20.8 1.0 fusion.63
  21.8 12.1 %all_gather.32 = bf16[256,1024]{1,0:T(8,128)(2,1)S(1)} all-gather(bf16[256,256]{1,0:T(8,128)(2,1)S(1)} %fusion.63), channel_id=1, replica_groups=mesh['sp'=8,'tp'=4] {'tp'}, dimensions={1}, use_global_device_ids=true | all-gather | bytes 655360 | tf_op jit(solution)/shard_map/all_gather | solution.py:16
  34.0 0.8 fusion.81
  34.8 1.0 fusion.53
  35.8 5.7 %fusion.10 = f32[64,64,4,4,12]{1,4,3,2,0:T(8,128)} fusion(f32[64,64,4,15]{1,3,2,0:T(8,128)S(1)} %fusion.53, s32[4,12]{1,0:T(4,128)S(1)} %subtract_add_fusion.1), kind=kOutput, calls=%fused_computation.16 | convolution fusion | flops 141558480 | bytes 4128960 | tf_op jit(solution)/shard_map/hab,ria,qkb->rhqik/dot_general | solution.py:64
  41.5 2.1 slice_bitcast_fusion.2
  43.6 13.8 %all-gather.9.cloned.1.call-done = bf16[2,1024,256]{2,1,0:T(8,128)(2,1)} async-done(((bf16[2,128,256]{2,1,0:T(8,128)(2,1)}), bf16[2,1024,256]{2,1,0:T(8,128)(2,1)}) %all-gather.9.cloned.1.call-update) | async-done | bytes 1048592 | tf_op jit(solution)/shard_map/all_gather | solution.py:92
  57.4 2.1 slice_bitcast_fusion.4
  59.5 21.4 %all-gather.11.cloned.1.call-done = bf16[2,1024,256]{2,1,0:T(8,128)(2,1)} async-done(((bf16[2,128,256]{2,1,0:T(8,128)(2,1)}), bf16[2,1024,256]{2,1,0:T(8,128)(2,1)}) %all-gather.11.cloned.1.call-update) | async-done | bytes 1048592 | tf_op jit(solution)/shard_map/all_gather | solution.py:93
  80.9 2.1 slice_bitcast_fusion.3
  83.0 0.6 fusion.27
  83.6 2.1 collective-permute-start
  85.7 1.3 collective-permute-start.1
  87.0 9.8 %copy.29 = f32[64,64,4,4,12]{0,1,3,4,2:T(8,128)} copy(f32[64,64,4,4,12]{1,4,3,2,0:T(8,128)} %fusion.10) | data formatting | bytes 6291456 | tf_op jit(solution)/shard_map/hab,ria,qkb->rhqik/dot_general | solution.py:64
  96.8 0.2 broadcast_and_fusion
  97.5 0.3 reshape.205
  97.8 0.3 reshape.204
  98.1 4.5 %fusion.82 = (f32[4,4,64]{2,0,1:T(4,128)S(1)}, f32[4,4,64,12,64]{2,4,0,3,1:T(8,128)S(1)}) fusion(f32[64,64,4,4,12]{0,1,3,4,2:T(8,128)} %copy.29, bf16[4,64,4,64,1]{3,2,1,0,4:T(4,128)(2,1)S(1)} %bitcast.104, bf16[12,64,4,64,1]{3,2,1,0,4:T(4,128)(2,1)S(1)} %bitcast.102, pred[4,64,12,64]{1,3,0,2:T(8,128)(4,1)S(1)} %broadcast_and_fusion), kind=kOutput, calls=%fused_computation.106 | convolution fusion | flops 103808000 | bytes 7016448 | tf_op jit(solution)/shard_map/rqhd,ikhd->rhqik/dot_general | solution.py:71
  102.7 1.0 fusion.2
  103.7 1.2 fusion.44
  105.3 1.3 all-gather.15.cloned.1.call-done
  106.6 2.1 fusion.36
  108.8 1.0 fusion.51
  109.8 24.7 %reduce-scatter.3.cloned.1.call-done = bf16[256,256]{0,1:T(8,128)(2,1)} async-done(((bf16[1024,256]{0,1:T(8,128)(2,1)}), bf16[256,256]{0,1:T(8,128)(2,1)}) %reduce-scatter.3.cloned.1.call-update) | async-done | bytes 131088 | tf_op jit(solution)/shard_map/reduce_scatter | solution.py:38
  134.5 1.0 fusion.64
  135.5 8.0 %all-gather.3 = f32[4,1,256]{2,1,0:T(1,128)S(1)} all-gather(f32[1,1,256]{2,1,0:T(1,128)S(1)} %bitcast.114), channel_id=3, replica_groups=mesh['sp'=8,'tp'=4] {'tp'}, dimensions={0}, use_global_device_ids=true | all-gather | bytes 5120 | tf_op jit(solution)/shard_map/all_gather | solution.py:105
  143.6 1.0 fusion.69
  144.6 11.4 %all_gather.39 = bf16[256,1024]{1,0:T(8,128)(2,1)S(1)} all-gather(bf16[256,256]{1,0:T(8,128)(2,1)S(1)} %fusion.69), channel_id=1, replica_groups=mesh['sp'=8,'tp'=4] {'tp'}, dimensions={1}, use_global_device_ids=true | all-gather | bytes 655360 | tf_op jit(solution)/shard_map/all_gather | solution.py:16
  156.0 2.0 fusion.24
  158.0 1.3 collective-permute-start.2
  159.3 1.3 collective-permute-start.3
  160.6 5.7 %fusion.8 = f32[64,64,4,4,12]{1,4,3,2,0:T(8,128)} fusion(f32[64,64,4,15]{1,3,2,0:T(8,128)S(1)} %fusion.51, s32[4,12]{1,0:T(4,128)S(1)} %subtract_add_fusion.1), kind=kOutput, calls=%fused_computation.14 | convolution fusion | flops 141558480 | bytes 4128960 | tf_op jit(solution)/shard_map/hab,ria,qkb->rhqik/dot_general | solution.py:64
  166.2 9.8 %copy.36 = f32[64,64,4,4,12]{0,1,3,4,2:T(8,128)} copy(f32[64,64,4,4,12]{1,4,3,2,0:T(8,128)} %fusion.8) | data formatting | bytes 6291456 | tf_op jit(solution)/shard_map/hab,ria,qkb->rhqik/dot_general | solution.py:64
  176.2 1.0 pad_maximum_fusion.1
  177.3 0.3 reshape.210
  177.7 0.3 reshape.209
  178.0 4.5 %fusion.83 = (f32[4,4,64]{2,0,1:T(4,128)S(1)}, f32[4,4,64,12,64]{2,4,0,3,1:T(8,128)S(1)}) fusion(f32[64,64,4,4,12]{0,1,3,4,2:T(8,128)} %copy.36, bf16[4,64,4,64,1]{3,2,1,0,4:T(4,128)(2,1)S(1)} %bitcast.103, bf16[12,64,4,64,1]{3,2,1,0,4:T(4,128)(2,1)S(1)} %bitcast.101, pred[4,64,12,64]{1,3,0,2:T(8,128)(4,1)S(1)} %broadcast_and_fusion), kind=kOutput, calls=%fused_computation.107 | convolution fusion | flops 103808000 | bytes 7016448 | tf_op jit(solution)/shard_map/rqhd,ikhd->rhqik/dot_general | solution.py:71
  182.5 1.0 fusion.3
  183.6 1.2 fusion.47
  185.2 1.1 fusion.37
  186.3 28.2 %reduce-scatter.5.cloned.1.call-done = bf16[256,256]{0,1:T(8,128)(2,1)} async-done(((bf16[1024,256]{0,1:T(8,128)(2,1)}), bf16[256,256]{0,1:T(8,128)(2,1)}) %reduce-scatter.5.cloned.1.call-update) | async-done | bytes 131088 | tf_op jit(solution)/shard_map/reduce_scatter | solution.py:38
  (40 shorter events, 1.9 us)
Async XLA Ops:
  6.5 34.9 %all-gather.13.cloned.1.call-start = ((), (), s32[]{:S(2)}) async-start(), calls=%async_computation.4 | async-start | bytes 1179648 | tf_op jit(solution)/shard_map/all_gather | solution.py:94
  7.3 50.2 %all-gather.9.cloned.1.call-start = ((), (), s32[]{:S(2)}) async-start(), calls=%async_computation.2 | async-start | bytes 1179648 | tf_op jit(solution)/shard_map/all_gather | solution.py:92
  8.0 72.9 %all-gather.11.cloned.1.call-start = ((), (), s32[]{:S(2)}) async-start(), calls=%async_computation.3 | async-start | bytes 1179648 | tf_op jit(solution)/shard_map/all_gather | solution.py:93
  8.7 97.9 %all-gather.15.cloned.1.call-start = ((), (), s32[]{:S(2)}) async-start(), calls=%async_computation.5 | async-start | bytes 1179648 | tf_op jit(solution)/shard_map/all_gather | solution.py:95
  9.3 125.2 %reduce-scatter.3.cloned.1.call-start = ((), (), s32[]{:S(2)}) async-start(), calls=%async_computation.6 | async-start | bytes 655360 | tf_op jit(solution)/shard_map/reduce_scatter | solution.py:38
  83.6 13.7 %collective-permute-start = (bf16[4,64,512]{2,1,0:T(8,128)(2,1)S(1)}, bf16[4,64,512]{2,1,0:T(8,128)(2,1)S(1)}, u32[]{:S(2)}, u32[]{:S(2)}) collective-permute-start(bf16[4,64,512]{2,1,0:T(8,128)(2,1)S(1)} %bitcast.105), channel_id=1, source_target_pairs={{0,4},{4,8},{8,12},{12,16},{16,20},{20,24},{24,28},{1,5},{5,9},{9,... | collective-permute-start | bytes 786440 | tf_op jit(solution)/shard_map/ppermute | solution.py:27
  85.7 11.6 %collective-permute-start.1 = (bf16[4,64,512]{2,1,0:T(8,128)(2,1)S(1)}, bf16[4,64,512]{2,1,0:T(8,128)(2,1)S(1)}, u32[]{:S(2)}, u32[]{:S(2)}) collective-permute-start(bf16[4,64,512]{2,1,0:T(8,128)(2,1)S(1)} %bitcast.106), channel_id=1, source_target_pairs={{4,0},{8,4},{12,8},{16,12},{20,16},{24,20},{28,24},{5,1},{9,5},{13... | collective-permute-start | bytes 786440 | tf_op jit(solution)/shard_map/ppermute | solution.py:30
  108.8 105.7 %reduce-scatter.5.cloned.1.call-start = ((), (), s32[]{:S(2)}) async-start(), calls=%async_computation.7 | async-start | bytes 655360 | tf_op jit(solution)/shard_map/reduce_scatter | solution.py:38
  158.0 18.2 %collective-permute-start.2 = (bf16[4,64,512]{2,1,0:T(8,128)(2,1)S(1)}, bf16[4,64,512]{2,1,0:T(8,128)(2,1)S(1)}, u32[]{:S(2)}, u32[]{:S(2)}) collective-permute-start(bf16[4,64,512]{2,1,0:T(8,128)(2,1)S(1)} %bitcast.108), channel_id=1, source_target_pairs={{0,4},{4,8},{8,12},{12,16},{16,20},{20,24},{24,28},{1,5},{5,9},{9,... | collective-permute-start | bytes 786440 | tf_op jit(solution)/shard_map/ppermute | solution.py:27
  159.3 16.9 %collective-permute-start.3 = (bf16[4,64,512]{2,1,0:T(8,128)(2,1)S(1)}, bf16[4,64,512]{2,1,0:T(8,128)(2,1)}, u32[]{:S(2)}, u32[]{:S(2)}) collective-permute-start(bf16[4,64,512]{2,1,0:T(8,128)(2,1)S(1)} %bitcast.109), channel_id=1, source_target_pairs={{4,0},{8,4},{12,8},{16,12},{20,16},{24,20},{28,24},{5,1},{9,5},{13... | collective-permute-start | bytes 786440 | tf_op jit(solution)/shard_map/ppermute | solution.py:30
  183.5 1.6 copy-start
Sparse Core Ops, SparseCore 0:
  8.9 24.9 all-gather.12
  35.5 21.8 all-gather.8
  59.0 21.8 all-gather.10
  82.3 24.2 all-gather.14
  109.3 25.1 reduce-scatter.2
  186.4 28.0 reduce-scatter.4
